TPU v7x, 32 devices: a whole 2x2x4 slice. The times are simulated.
32 devices in a mesh: ep: 32 (over z, y, x, core).
Axes of the slice: x: 2, y: 2, z: 4, core: 2. Of those that a mesh axis runs over, the one named last changes fastest.
Arguments:
- hidden_in: bfloat16 [64, 2048], P('ep'), may hold values from -6 to 6
- lengths: int32 [64], P('ep'), may hold values from 1 to 1024, as said below
- key_cache: bfloat16 [64, 1024, 512], P('ep'), may hold values from -30 to 30
- value_cache: bfloat16 [64, 1024, 512], P('ep'), may hold values from -6 to 6
- query_w: bfloat16 [2048, 2048], P('ep'), may hold values from -0.125 to 0.125
- key_w: bfloat16 [2048, 512], P('ep'), may hold values from -0.125 to 0.125
- value_w: bfloat16 [2048, 512], P('ep'), may hold values from -0.125 to 0.125
- out_w: bfloat16 [2048, 2048], P('ep'), may hold values from -0.125 to 0.125
- lam_heads: float32 [8], replicated, may hold values from 0.3 to 0.8
- head_gain: float32 [256], replicated, may hold values from 0.1 to 1.9
- attn_gain: float32 [2048], replicated, may hold values from 0.1 to 1.9
- moe_gain: float32 [2048], replicated, may hold values from 0.1 to 1.9
- routing: int32 [64, 6], replicated, may hold values from 0 to 31, all different within a row; in each aligned block of 64 rows (0 to 63, 64 to 127, ...) at most 24 rows name the same one
- route_weight: float32 [64, 6], replicated, may hold values from 0.1 to 0.6
- gate_w: bfloat16 [32, 2048, 512], P('ep'), may hold values from -0.125 to 0.125
- up_w: bfloat16 [32, 2048, 512], P('ep'), may hold values from -0.125 to 0.125
- down_w: bfloat16 [32, 512, 2048], P('ep'), may hold values from -0.25 to 0.25
- shared_gate: bfloat16 [2048, 512], replicated, may hold values from -0.125 to 0.125
- shared_up: bfloat16 [2048, 512], replicated, may hold values from -0.125 to 0.125
- shared_down: bfloat16 [512, 2048], replicated, may hold values from -0.25 to 0.25
Outputs:
- layer_out: bfloat16 [64, 2048], P('ep')
- key_new: bfloat16 [64, 512], P('ep')
- value_new: bfloat16 [64, 512], P('ep')
Inputs may be any that keep to these rules, and one draw needn't show every extreme that they name: `lengths`: some sequence has exactly 1024 positions in use. `routing`: each row names 6 different experts; no expert is named by more than 24 rows, a bound that some block reaches.
All inputs are finite; a program needn't handle non-finite values.
Results may differ from a plain program's by a relative error of at most 0.013.
The roundings to bfloat16 on the way count: a program that leaves them out, or rounds other values in their place, can miss the bound.
Values may be sent and summed in bfloat16 or wider, within the bound.
A program may use at most 64 MiB of HBM per device.

v0:
```python
import jax
import jax.numpy as jnp
from jax import lax
from jax.sharding import PartitionSpec as P

KV_HEADS = 2
HEAD_DIM = 128
EXP_CAP = 24
eps_norm = 1e-06
eps_head = 1e-05
theta_base = 500000.0


def rms_scale(row_block, gain_vec, epsilon):
    row_block = row_block.astype(jnp.float32)
    return (
        row_block
        * lax.rsqrt(jnp.mean(row_block * row_block, axis=-1, keepdims=True) + epsilon)
        * gain_vec
    )


def rotate(vectors, positions):
    half_width = vectors.shape[-1] // 2
    inverse = theta_base ** (-jnp.arange(half_width, dtype=jnp.float32) / half_width)
    angles = positions.astype(jnp.float32)[..., None] * inverse
    cosine, sine_part = (jnp.cos(angles), jnp.sin(angles))
    lower_half, upper_half = (vectors[..., :half_width], vectors[..., half_width:])
    return jnp.concatenate(
        [
            lower_half * cosine - upper_half * sine_part,
            lower_half * sine_part + upper_half * cosine,
        ],
        axis=-1,
    )


def attend(queries, key_new, value_new, cache_keys, cache_values, lengths, lam_heads, head_gain):
    num_seqs, kv_heads, group_size = (queries.shape[0], queries.shape[1], queries.shape[2])
    head_dim = queries.shape[-1]
    cache_len = cache_keys.shape[1]
    cache_keys = cache_keys.reshape(num_seqs, cache_len, kv_heads, 2, head_dim)
    cache_values = cache_values.reshape(num_seqs, cache_len, kv_heads, -1)
    value_new = value_new.reshape(num_seqs, kv_heads, -1)
    score_scale = head_dim ** (-0.5)
    scores = (
        jnp.einsum("skgph,sckph->skgpc", queries, cache_keys, preferred_element_type=jnp.float32)
        * score_scale
    )
    self_score = (
        jnp.einsum("skgph,skph->skgp", queries, key_new, preferred_element_type=jnp.float32)
        * score_scale
    )
    live_mask = (jnp.arange(cache_len)[None, :] < lengths[:, None])[:, None, None, None, :]
    peak = jnp.maximum(jnp.max(jnp.where(live_mask, scores, -jnp.inf), axis=-1), self_score)
    weights = jnp.where(live_mask, jnp.exp(scores - peak[..., None]), 0.0)
    self_weight = jnp.exp(self_score - peak)
    totals = jnp.sum(weights, axis=-1) + self_weight
    lambda_grid = lam_heads.reshape(kv_heads, group_size)[None]
    combined = (
        weights[:, :, :, 0] / totals[:, :, :, 0, None]
        - lambda_grid[..., None] * weights[:, :, :, 1] / totals[:, :, :, 1, None]
    ).astype(jnp.bfloat16)
    self_combined = (
        self_weight[..., 0] / totals[..., 0] - lambda_grid * self_weight[..., 1] / totals[..., 1]
    ).astype(jnp.bfloat16)
    head_out = jnp.einsum(
        "skgc,sckv->skgv", combined, cache_values, preferred_element_type=jnp.float32
    )
    head_out = (
        head_out
        + self_combined.astype(jnp.float32)[..., None]
        * value_new.astype(jnp.float32)[:, :, None, :]
    )
    return rms_scale(head_out, head_gain, eps_head).astype(jnp.bfloat16).reshape(num_seqs, -1)


def expert_rows(row_block, routed_here, gate_one, up_one, down_one):
    slot_index = jnp.cumsum(routed_here) - 1
    pick_table = (
        (slot_index[None, :] == jnp.arange(EXP_CAP)[:, None]) & (routed_here[None, :] > 0)
    ).astype(jnp.bfloat16)
    picked = jnp.dot(pick_table, row_block, preferred_element_type=jnp.float32).astype(jnp.bfloat16)
    hidden = (
        jax.nn.silu(jnp.dot(picked, gate_one, preferred_element_type=jnp.float32))
        * jnp.dot(picked, up_one, preferred_element_type=jnp.float32)
    ).astype(jnp.bfloat16)
    result = jnp.dot(hidden, down_one, preferred_element_type=jnp.float32).astype(jnp.bfloat16)
    return jnp.dot(pick_table.T, result, preferred_element_type=jnp.float32)


def on_device(
    hidden_in,
    lengths,
    key_cache,
    value_cache,
    query_w,
    key_w,
    value_w,
    out_w,
    lam_heads,
    head_gain,
    attn_gain,
    moe_gain,
    routing,
    route_weight,
    gate_w,
    up_w,
    down_w,
    shared_gate,
    shared_up,
    shared_down,
):
    device = lax.axis_index("ep")
    tok_dev = hidden_in.shape[0]
    all_rows = lax.all_gather(hidden_in, "ep", axis=0, tiled=True)
    normed = rms_scale(all_rows, attn_gain, eps_norm).astype(jnp.bfloat16)
    joined_rows = jnp.concatenate([query_w, key_w, value_w], axis=1)
    column_block = lax.all_to_all(joined_rows, "ep", split_axis=1, concat_axis=0, tiled=True)
    column_sums = jnp.dot(normed, column_block, preferred_element_type=jnp.float32)
    projected = lax.all_to_all(column_sums, "ep", split_axis=0, concat_axis=1, tiled=True)
    query_cols = query_w.shape[1]
    key_cols = key_w.shape[1]
    queries = rotate(
        projected[:, :query_cols].reshape(tok_dev, KV_HEADS, -1, 2, HEAD_DIM),
        lengths[:, None, None, None],
    ).astype(jnp.bfloat16)
    key_new = rotate(
        projected[:, query_cols : query_cols + key_cols].reshape(tok_dev, KV_HEADS, 2, HEAD_DIM),
        lengths[:, None, None],
    ).astype(jnp.bfloat16)
    value_new = projected[:, query_cols + key_cols :].astype(jnp.bfloat16)
    attn_out = attend(
        queries, key_new, value_new, key_cache, value_cache, lengths, lam_heads, head_gain
    )
    pieces = lax.all_to_all(attn_out, "ep", split_axis=1, concat_axis=0, tiled=True)
    routed_here = jnp.sum((routing == device).astype(jnp.int32), axis=1)
    partial_value = jnp.dot(pieces, out_w, preferred_element_type=jnp.float32)
    attn_proj = lax.psum(partial_value, "ep").astype(jnp.bfloat16)
    mixer_all = (all_rows.astype(jnp.float32) + attn_proj.astype(jnp.float32)).astype(jnp.bfloat16)
    moe_all = rms_scale(mixer_all, moe_gain, eps_norm).astype(jnp.bfloat16)
    weight_col = jnp.sum(jnp.where(routing == device, route_weight, 0.0), axis=1)
    spread_back = (
        expert_rows(moe_all, routed_here, gate_w[0], up_w[0], down_w[0]) * weight_col[:, None]
    )
    routed = lax.psum_scatter(spread_back, "ep", scatter_dimension=0, tiled=True)
    after_mixer = lax.dynamic_slice_in_dim(mixer_all, device * tok_dev, tok_dev, 0)
    moe_in = lax.dynamic_slice_in_dim(moe_all, device * tok_dev, tok_dev, 0)
    shared_hidden = (
        jax.nn.silu(jnp.dot(moe_in, shared_gate, preferred_element_type=jnp.float32))
        * jnp.dot(moe_in, shared_up, preferred_element_type=jnp.float32)
    ).astype(jnp.bfloat16)
    shared_out = jnp.dot(shared_hidden, shared_down, preferred_element_type=jnp.float32)
    layer_out = (after_mixer.astype(jnp.float32) + routed + shared_out).astype(jnp.bfloat16)
    return (layer_out, key_new.reshape(tok_dev, -1), value_new)


def solution(mesh):
    placed = (
        P("ep", None),
        P("ep"),
        P("ep", None, None),
        P("ep", None, None),
        P("ep", None),
        P("ep", None),
        P("ep", None),
        P("ep", None),
        P(),
        P(),
        P(),
        P(),
        P(),
        P(),
        P("ep", None, None),
        P("ep", None, None),
        P("ep", None, None),
        P(),
        P(),
        P(),
    )
    return jax.shard_map(
        on_device,
        mesh=mesh,
        in_specs=placed,
        out_specs=(P("ep", None), P("ep", None), P("ep", None)),
        check_vma=False,
    )
```

profile of v0, /device:TPU:0, one launch (start us, length us, event | category | flops | bytes accessed | tf_op | source)
XLA Modules:
  0.0 275.9 jit_solution(12402558321039086071)
XLA Ops:
  7.2 1.2 pad_maximum_fusion
  8.4 0.5 all_to_all.40
  9.0 1.0 copy.52
  9.9 7.3 %all-to-all-start = ((bf16[64,32,96]{2,0,1:T(8,128)(2,1)}), bf16[64,32,96]{2,0,1:T(8,128)(2,1)S(1)}, u32[]{:S(2)}, u32[]{:S(2)}) async-start(bf16[64,32,96]{2,0,1:T(8,128)(2,1)} %copy.52), calls=%async_computation | async-start | bytes 1048576 | tf_op jit(solution)/shard_map/all_to_all | solution.py:119
  17.5 44.4 %all-gather = bf16[32,2,2048]{2,1,0:T(2,128)(2,1)S(1)} all-gather(bf16[1,2,2048]{2,1,0:T(2,128)(2,1)S(1)} %bitcast.88), channel_id=1, replica_groups=mesh['ep'=32] {'ep'}, dimensions={0}, use_global_device_ids=true | all-gather | bytes 270336 | tf_op jit(solution)/shard_map/all_gather | solution.py:116
  62.0 0.1 multiply_reduce_fusion
  62.1 0.8 multiply_convert_fusion
  62.9 1.1 dot_general.41
  64.4 0.2 fusion.32
  64.6 0.6 copy.55
  65.3 2.6 all-to-all-start.1
  68.0 4.0 %reshape.245 = bf16[2,1024,2,2,128]{4,3,2,1,0:T(2,128)(2,1)} reshape(bf16[2,1024,512]{2,1,0:T(8,128)(2,1)} %param.22) | data formatting | bytes 4194304 | tf_op jit(solution)/shard_map/reshape | solution.py:42
  72.0 3.1 %all-to-all-done.1 = f32[32,2,96]{2,1,0:T(2,128)S(1)} async-done(((f32[32,2,96]{2,1,0:T(2,128)}), f32[32,2,96]{2,1,0:T(2,128)S(1)}, u32[]{:S(2)}, u32[]{:S(2)}) %all-to-all-start.1) | async-done | bytes 24608 | tf_op jit(solution)/shard_map/all_to_all | solution.py:121
  75.6 0.2 fusion.51
  75.8 2.5 select_reduce_fusion
  78.3 0.2 fusion.66
  78.6 0.5 multiply_reduce_fusion.1
  79.3 0.6 copy.62
  79.9 2.7 all-to-all-start.2
  82.8 0.6 convert_element_type.102
  83.4 6.5 %all-to-all-done.2 = bf16[2,32,64]{2,0,1:T(2,128)(2,1)S(1)} async-done(((bf16[2,32,64]{2,0,1:T(2,128)(2,1)}), bf16[2,32,64]{2,0,1:T(2,128)(2,1)S(1)}, u32[]{:S(2)}, u32[]{:S(2)}) %all-to-all-start.2) | async-done | bytes 8224 | tf_op jit(solution)/shard_map/all_to_all | solution.py:136
  89.8 0.2 fusion.68
  90.1 43.0 %all-reduce.5 = bf16[64,2048]{1,0:T(8,128)(2,1)S(1)} all-reduce(f32[64,2048]{1,0:T(8,128)S(1)} %fusion.68), channel_id=1, replica_groups=mesh['ep'=32] {'ep'}, use_global_device_ids=true, to_apply=%region_4.5 | all-reduce | flops 131072 | bytes 786432 | tf_op jit(solution)/shard_map/psum | solution.py:139
  133.0 0.2 fusion.29
  133.2 0.1 fusion.31
  133.4 0.2 convolution_convert_fusion.1
  133.5 2.1 fusion.7
  135.6 0.4 fusion.22
  136.0 1.4 convolution_multiply_fusion
  137.4 2.0 fusion.55
  139.4 126.1 %all-reduce.4.cloned.1.call-done = f32[64,2048]{1,0:T(8,128)} async-done(((f32[64,2048]{1,0:T(8,128)}), f32[64,2048]{1,0:T(8,128)}) %all-reduce.4.cloned.1.call-update) | async-done | bytes 524304
  265.5 3.6 %fusion = bf16[2,2048]{1,0:T(2,128)(2,1)} fusion(bf16[512,2048]{1,0:T(8,128)(2,1)} %param.39, bf16[2048,512]{1,0:T(8,128)(2,1)} %param.38, f32[64,2048]{1,0:T(8,128)} %all-reduce.4.cloned.1.call-done, u32[]{:T(128)S(6)} %multiply.28, bf16[64,2048]{1,0:T(8,128)(2,1)S(1)} %get-tuple-element.6, s32[]{:T(128)S(6)} %select_n.17, f32[2,512]{1,0:T(2,128)S(1)} %fusion.55, ...), kind=kOutput, calls=%fused_computation.4 | convolution fusion | flops 8411136 | bytes 4240896 | tf_op jit(solution)/shard_map/dot_general | solution.py:153
  (62 shorter events, 1.6 us)
Async XLA Ops:
  7.2 128.9 %copy-start = (bf16[1,512,2048]{2,1,0:T(8,128)(2,1)S(1)}, bf16[1,512,2048]{2,1,0:T(8,128)(2,1)}, u32[]{:S(2)}) copy-start(bf16[1,512,2048]{2,1,0:T(8,128)(2,1)} %param.36) | copy-start | bytes 6291460
  7.2 10.1 %copy-start.10 = (s32[2]{0:T(128)S(1)}, s32[2]{0:T(128)}, u32[]{:S(2)}) copy-start(s32[2]{0:T(128)} %param.21) | copy-start | bytes 28
  7.2 10.1 %copy-start.7 = (f32[64,6]{0,1:T(8,128)S(1)}, f32[64,6]{0,1:T(8,128)}, u32[]{:S(2)}) copy-start(f32[64,6]{0,1:T(8,128)} %param.33) | copy-start | bytes 4612
  7.2 10.1 %copy-start.8 = (s32[64,6]{0,1:T(8,128)S(1)}, s32[64,6]{0,1:T(8,128)}, u32[]{:S(2)}) copy-start(s32[64,6]{0,1:T(8,128)} %param.32) | copy-start | bytes 4612
  7.2 10.3 %copy-start.5 = (bf16[2,2048]{1,0:T(2,128)(2,1)S(1)}, bf16[2,2048]{1,0:T(2,128)(2,1)}, u32[]{:S(2)}) copy-start(bf16[2,2048]{1,0:T(2,128)(2,1)} %param.20) | copy-start | bytes 24580
  8.9 53.2 %copy-start.3 = (f32[2048]{0:T(1024)S(1)}, f32[2048]{0:T(1024)}, u32[]{:S(2)}) copy-start(f32[2048]{0:T(1024)} %param.30) | copy-start | bytes 24580
  9.9 54.4 %all-to-all-start = ((bf16[64,32,96]{2,0,1:T(8,128)(2,1)}), bf16[64,32,96]{2,0,1:T(8,128)(2,1)S(1)}, u32[]{:S(2)}, u32[]{:S(2)}) async-start(bf16[64,32,96]{2,0,1:T(8,128)(2,1)} %copy.52), calls=%async_computation | async-start | bytes 1048576 | tf_op jit(solution)/shard_map/all_to_all | solution.py:119
  17.3 50.7 %copy-start.12 = (f32[8]{0:T(128)S(1)}, f32[8]{0:T(128)}, u32[]{:S(2)}) copy-start(f32[8]{0:T(128)} %param.28) | copy-start | bytes 100
  65.3 9.8 %all-to-all-start.1 = ((f32[32,2,96]{2,1,0:T(2,128)}), f32[32,2,96]{2,1,0:T(2,128)S(1)}, u32[]{:S(2)}, u32[]{:S(2)}) async-start(f32[32,2,96]{2,1,0:T(2,128)} %copy.55), calls=%async_computation.1 | async-start | bytes 65536 | tf_op jit(solution)/shard_map/all_to_all | solution.py:121
  75.2 3.9 %copy-start.6 = (bf16[2,512]{1,0:T(2,128)(2,1)}, bf16[2,512]{1,0:T(2,128)(2,1)S(1)}, u32[]{:S(2)}) copy-start(bf16[2,512]{1,0:T(2,128)(2,1)S(1)} %slice.101) | copy-start | bytes 6148
  75.3 3.3 %copy-start.11 = (bf16[2,1024,512]{2,1,0:T(8,128)(2,1)S(1)}, bf16[2,1024,512]{2,1,0:T(8,128)(2,1)}, u32[]{:S(2)}) copy-start(bf16[2,1024,512]{2,1,0:T(8,128)(2,1)} %param.23) | copy-start | bytes 6291460
  78.3 0.8 copy-start.9
  78.3 11.6 %copy-start.2 = (bf16[64,2048]{1,0:T(8,128)(2,1)S(1)}, bf16[64,2048]{1,0:T(8,128)(2,1)}, u32[]{:S(2)}) copy-start(bf16[64,2048]{1,0:T(8,128)(2,1)} %param.27) | copy-start | bytes 786436
  79.1 54.1 %copy-start.4 = (f32[2048]{0:T(1024)S(1)}, f32[2048]{0:T(1024)}, u32[]{:S(2)}) copy-start(f32[2048]{0:T(1024)} %param.31) | copy-start | bytes 24580
  79.9 9.9 %all-to-all-start.2 = ((bf16[2,32,64]{2,0,1:T(2,128)(2,1)}), bf16[2,32,64]{2,0,1:T(2,128)(2,1)S(1)}, u32[]{:S(2)}, u32[]{:S(2)}) async-start(bf16[2,32,64]{2,0,1:T(2,128)(2,1)} %copy.62), calls=%async_computation.2 | async-start | bytes 32768 | tf_op jit(solution)/shard_map/all_to_all | solution.py:136
  82.7 182.9 %all-reduce.4.cloned.1.call-start = ((), (), s32[]{:S(2)}) async-start(), calls=%async_computation.3 | async-start | bytes 1048576
  133.0 2.6 copy-start.1
Sparse Core Ops, SparseCore 0:
  137.5 127.9 all-reduce.3
where the time goes:
time: 276 us
  waiting for transfers between devices  136 us (49%)
  blocking collectives  87.4 us (32%)
  between operations  14.4 us (5%)
  matrix products  13.2 us (5%)
  starting transfers between devices  12.7 us (5%)
  local copies, waits for them, and re-layouts  9.12 us (3%)
  other arithmetic  3.5 us (1%)
    unnamed x2, waiting for transfers between devices  126 us
    all_gather x1, blocking collectives, on_device(): all_rows = lax.all_gather(hidden_in, 'ep', axis=0, tiled=True)  44.4 us
    psum x1, blocking collectives, on_device(): attn_proj = lax.psum(partial_value, 'ep').astype(jnp.bfloat16)  43 us
    all_to_all x1, starting transfers between devices, on_device(): lax.all_to_all(joined_rows, 'ep', split_axis=1, concat_axis=0, tiled=True)  7.33 us
    all_to_all x1, waiting for transfers between devices, on_device(): lax.all_to_all(attn_out, 'ep', split_axis=1, concat_axis=0, tiled=True)  6.46 us
  transfers between devices with their start and end apart: 4, of which 3 were waited for; matrix products, arithmetic and copies ran while one was open for 3% of the time, Pallas kernels for 0%

commit v1 on v0

--- a/solution.py
+++ b/solution.py
@@ -136,7 +136,7 @@
     pieces = lax.all_to_all(attn_out, "ep", split_axis=1, concat_axis=0, tiled=True)
     routed_here = jnp.sum((routing == device).astype(jnp.int32), axis=1)
     partial_value = jnp.dot(pieces, out_w, preferred_element_type=jnp.float32)
-    attn_proj = lax.psum(partial_value, "ep").astype(jnp.bfloat16)
+    attn_proj = jnp.sum(lax.all_gather(partial_value, "ep"), axis=0).astype(jnp.bfloat16)
     mixer_all = (all_rows.astype(jnp.float32) + attn_proj.astype(jnp.float32)).astype(jnp.bfloat16)
     moe_all = rms_scale(mixer_all, moe_gain, eps_norm).astype(jnp.bfloat16)
     weight_col = jnp.sum(jnp.where(routing == device, route_weight, 0.0), axis=1)

time: 276 us -> 352 us (1.28)
  waiting for transfers between devices: 136 us -> 238 us
  blocking collectives: 87.4 us -> 54.4 us
  other arithmetic: 3.5 us -> 10.4 us
    all_gather x0 -> x1, waiting for transfers between devices: none -> 110 us  [on_device(): lax.all_gather(partial_value, 'ep')]
    psum x1 -> x0, blocking collectives: 43 us -> none  [on_device(): attn_proj = lax.psum(partial_value, 'ep').astype(jnp.bfloat16)]
    all_to_all x0 -> x1, blocking collectives: none -> 9.79 us  [on_device(): lax.all_to_all(attn_out, 'ep', split_axis=1, concat_axis=0, tiled=True)]
    reduce_sum x0 -> x1, other arithmetic: none -> 6.91 us  [on_device(): jnp.sum(lax.all_gather(partial_value, 'ep'), axis=0).astype(jnp.bfloat16)]
    all_to_all x1 -> x0, waiting for transfers between devices: 6.46 us -> none  [on_device(): lax.all_to_all(attn_out, 'ep', split_axis=1, concat_axis=0, tiled=True)]
    unnamed x2 -> x3, waiting for transfers between devices: 126 us -> 126 us
where the time goes in v1:
time: 352 us; the launch traced here: 351 us
  waiting for transfers between devices  238 us (68%)
  blocking collectives  54.4 us (15%)
  matrix products  15.5 us (4%)
  between operations  14.3 us (4%)
  other arithmetic  10.4 us (3%)
  starting transfers between devices  9.96 us (3%)
  local copies, waits for them, and re-layouts  8.52 us (2%)
    unnamed x3, waiting for transfers between devices  126 us
    all_gather x1, waiting for transfers between devices, on_device(): lax.all_gather(partial_value, 'ep')  110 us
    all_gather x1, blocking collectives, on_device(): all_rows = lax.all_gather(hidden_in, 'ep', axis=0, tiled=True)  44.6 us
    all_to_all x1, blocking collectives, on_device(): lax.all_to_all(attn_out, 'ep', split_axis=1, concat_axis=0, tiled=True)  9.79 us
    all_to_all x1, starting transfers between devices, on_device(): lax.all_to_all(joined_rows, 'ep', split_axis=1, concat_axis=0, tiled=True)  7.33 us
  transfers between devices with their start and end apart: 4, of which 3 were waited for; matrix products, arithmetic and copies ran while one was open for 3% of the time, Pallas kernels for 0%

profile of v1, /device:TPU:0, one launch (start us, length us, event | category | flops | bytes accessed | tf_op | source)
XLA Modules:
  0.0 351.4 jit_solution(2941904773761426140)
XLA Ops:
  7.2 1.2 pad_maximum_fusion
  8.4 0.5 all_to_all.40
  8.9 1.0 copy.52
  9.9 7.3 %all-to-all-start = ((bf16[64,32,96]{2,0,1:T(8,128)(2,1)}), bf16[64,32,96]{2,0,1:T(8,128)(2,1)S(1)}, u32[]{:S(2)}, u32[]{:S(2)}) async-start(bf16[64,32,96]{2,0,1:T(8,128)(2,1)} %copy.52), calls=%async_computation | async-start | bytes 1048576 | tf_op jit(solution)/shard_map/all_to_all | solution.py:119
  17.3 44.6 %all-gather.1 = bf16[32,2,2048]{2,1,0:T(2,128)(2,1)S(1)} all-gather(bf16[1,2,2048]{2,1,0:T(2,128)(2,1)S(1)} %bitcast.90), channel_id=1, replica_groups=mesh['ep'=32] {'ep'}, dimensions={0}, use_global_device_ids=true | all-gather | bytes 270336 | tf_op jit(solution)/shard_map/all_gather | solution.py:116
  61.9 0.1 multiply_reduce_fusion
  62.1 0.8 multiply_convert_fusion
  62.9 1.1 dot_general.41
  64.2 0.2 fusion.32
  64.4 0.6 copy.55
  65.1 2.6 all-to-all-start.1
  67.7 0.1 multiply_cosine_fusion
  67.8 4.0 %reshape.245 = bf16[2,1024,2,2,128]{4,3,2,1,0:T(2,128)(2,1)} reshape(bf16[2,1024,512]{2,1,0:T(8,128)(2,1)} %param.22) | data formatting | bytes 4194304 | tf_op jit(solution)/shard_map/reshape | solution.py:42
  71.8 3.0 all-to-all-done.1
  75.3 0.2 fusion.51
  75.5 2.4 select_reduce_fusion
  77.9 0.2 fusion.66
  78.2 2.1 multiply_reduce_fusion.1
  80.5 9.8 %all_to_all.54 = bf16[2,32,64]{2,0,1:T(2,128)(2,1)S(1)} all-to-all(bf16[2,32,64]{2,0,1:T(2,128)(2,1)S(1)} %copy.62), channel_id=1, replica_groups=mesh['ep'=32] {'ep'}, dimensions={1} | all-to-all | bytes 16384 | tf_op jit(solution)/shard_map/all_to_all | solution.py:136
  90.3 1.0 fusion.68
  91.9 0.6 convert_element_type.102
  92.5 109.8 %all-gather.4.cloned.1.call-done = f32[2048,2048]{1,0:T(8,128)} async-done(((f32[64,2048]{1,0:T(8,128)}), f32[2048,2048]{1,0:T(8,128)}) %all-gather.4.cloned.1.call-update) | async-done | bytes 16777232 | tf_op jit(solution)/shard_map/all_gather | solution.py:139
  202.2 6.9 %reduce_sum.66 = bf16[64,2048]{1,0:T(8,128)(2,1)S(1)} reduce(f32[32,64,2048]{2,1,0:T(8,128)} %bitcast.84, f32[]{:T(128)} %constant.15.clone.1), dimensions={0}, to_apply=%region_4.5 | reduce | flops 4063232 | bytes 17039364 | tf_op jit(solution)/shard_map/reduce_sum | solution.py:139
  209.2 0.2 fusion.29
  209.4 0.1 fusion.31
  209.5 0.2 convolution_convert_fusion.1
  209.7 2.1 fusion.7
  211.7 0.4 fusion.22
  212.2 1.4 convolution_multiply_fusion
  213.6 2.0 fusion.55
  215.5 125.5 %all-reduce.3.cloned.1.call-done = f32[64,2048]{1,0:T(8,128)} async-done(((f32[64,2048]{1,0:T(8,128)}), f32[64,2048]{1,0:T(8,128)}) %all-reduce.3.cloned.1.call-update) | async-done | bytes 524304
  341.0 3.6 %fusion = bf16[2,2048]{1,0:T(2,128)(2,1)} fusion(bf16[512,2048]{1,0:T(8,128)(2,1)} %param.39, bf16[2048,512]{1,0:T(8,128)(2,1)} %param.38, f32[64,2048]{1,0:T(8,128)} %all-reduce.3.cloned.1.call-done, u32[]{:T(128)S(6)} %multiply.28, bf16[64,2048]{1,0:T(8,128)(2,1)S(1)} %get-tuple-element.6, s32[]{:T(128)S(6)} %select_n.17, f32[2,512]{1,0:T(2,128)S(1)} %fusion.55, ...), kind=kOutput, calls=%fused_computation.4 | convolution fusion | flops 8411136 | bytes 4240896 | tf_op jit(solution)/shard_map/dot_general | solution.py:153
  (62 shorter events, 1.5 us)
Async XLA Ops:
  7.2 205.0 %copy-start = (bf16[1,512,2048]{2,1,0:T(8,128)(2,1)S(1)}, bf16[1,512,2048]{2,1,0:T(8,128)(2,1)}, u32[]{:S(2)}) copy-start(bf16[1,512,2048]{2,1,0:T(8,128)(2,1)} %param.36) | copy-start | bytes 6291460
  7.2 10.1 %copy-start.5 = (bf16[2,2048]{1,0:T(2,128)(2,1)S(1)}, bf16[2,2048]{1,0:T(2,128)(2,1)}, u32[]{:S(2)}) copy-start(bf16[2,2048]{1,0:T(2,128)(2,1)} %param.20) | copy-start | bytes 24580
  8.4 53.7 %copy-start.3 = (f32[2048]{0:T(1024)S(1)}, f32[2048]{0:T(1024)}, u32[]{:S(2)}) copy-start(f32[2048]{0:T(1024)} %param.30) | copy-start | bytes 24580
  9.9 54.1 %copy-start.10 = (s32[2]{0:T(128)S(1)}, s32[2]{0:T(128)}, u32[]{:S(2)}) copy-start(s32[2]{0:T(128)} %param.21) | copy-start | bytes 28
  9.9 54.2 %all-to-all-start = ((bf16[64,32,96]{2,0,1:T(8,128)(2,1)}), bf16[64,32,96]{2,0,1:T(8,128)(2,1)S(1)}, u32[]{:S(2)}, u32[]{:S(2)}) async-start(bf16[64,32,96]{2,0,1:T(8,128)(2,1)} %copy.52), calls=%async_computation | async-start | bytes 1048576 | tf_op jit(solution)/shard_map/all_to_all | solution.py:119
  65.1 9.8 %all-to-all-start.1 = ((f32[32,2,96]{2,1,0:T(2,128)}), f32[32,2,96]{2,1,0:T(2,128)S(1)}, u32[]{:S(2)}, u32[]{:S(2)}) async-start(f32[32,2,96]{2,1,0:T(2,128)} %copy.55), calls=%async_computation.1 | async-start | bytes 65536 | tf_op jit(solution)/shard_map/all_to_all | solution.py:121
  67.6 134.6 %all-gather.4.cloned.1.call-start = ((), (), s32[]{:S(2)}) async-start(), calls=%async_computation.3 | async-start | bytes 17301504 | tf_op jit(solution)/shard_map/all_gather | solution.py:139
  67.8 4.0 %copy-start.11 = (f32[8]{0:T(128)S(1)}, f32[8]{0:T(128)}, u32[]{:S(2)}) copy-start(f32[8]{0:T(128)} %param.28) | copy-start | bytes 100
  75.0 5.3 %copy-start.6 = (bf16[2,512]{1,0:T(2,128)(2,1)}, bf16[2,512]{1,0:T(2,128)(2,1)S(1)}, u32[]{:S(2)}) copy-start(bf16[2,512]{1,0:T(2,128)(2,1)S(1)} %slice.101) | copy-start | bytes 6148
  77.9 2.4 copy-start.9
  77.9 12.4 %copy-start.2 = (bf16[64,2048]{1,0:T(8,128)(2,1)S(1)}, bf16[64,2048]{1,0:T(8,128)(2,1)}, u32[]{:S(2)}) copy-start(bf16[64,2048]{1,0:T(8,128)(2,1)} %param.27) | copy-start | bytes 786436
  78.2 13.2 %copy-start.7 = (f32[64,6]{0,1:T(8,128)S(1)}, f32[64,6]{0,1:T(8,128)}, u32[]{:S(2)}) copy-start(f32[64,6]{0,1:T(8,128)} %param.33) | copy-start | bytes 4612
  78.2 13.2 %copy-start.8 = (s32[64,6]{0,1:T(8,128)S(1)}, s32[64,6]{0,1:T(8,128)}, u32[]{:S(2)}) copy-start(s32[64,6]{0,1:T(8,128)} %param.32) | copy-start | bytes 4612
  91.4 249.7 %all-reduce.3.cloned.1.call-start = ((), (), s32[]{:S(2)}) async-start(), calls=%async_computation.4 | async-start | bytes 1048576
  202.2 7.1 %copy-start.4 = (f32[2048]{0:T(1024)S(1)}, f32[2048]{0:T(1024)}, u32[]{:S(2)}) copy-start(f32[2048]{0:T(1024)} %param.31) | copy-start | bytes 24580
  209.1 2.6 copy-start.1
Sparse Core Ops, SparseCore 0:
  91.5 110.6 all-gather.3
  213.7 127.3 all-reduce.2
